TPU v7x, 256 devices: a 4x2x16 block of a 4x16x16 slice. The times are simulated.
256 devices in a mesh: grp: 2 (over y), fs: 16 (over z), tp: 8 (over x, core).
Axes of the slice: x: 4, y: 2, z: 16, core: 2. Of those that a mesh axis runs over, the one named last changes fastest.
The devices are a block of a 4x16x16 slice.
Arguments:
- tokens: bfloat16 [32768, 2048], P(('grp', 'fs', 'tp')), parts along dimension 0, may hold values from -12 to 12
- norm_gain: float32 [2048], replicated, may hold values from 0.1 to 1.9
- w_in: bfloat16 [2048, 8192], P('fs', 'tp'), may hold values from -0.125 to 0.125
- w_out: bfloat16 [8192, 2048], P('tp', 'fs'), may hold values from -0.0625 to 0.0625
Outputs:
- mixed: bfloat16 [32768, 2048], P(('grp', 'fs', 'tp')), parts along dimension 0
There are 2 independent parts, one for each index of `grp`. A program takes and returns all parts, laid end to end along the dimension named above; an argument that names none is the same for every part. Nothing has to cross between parts.
All inputs are finite; a program needn't handle non-finite values.
Results may differ from a plain program's by a relative error of at most 0.012.
Values may be sent and summed in bfloat16 or wider, within the bound.
No kernel may reach another device: no remote copies, remote signals or barrier semaphores. Data moves between devices by JAX's collectives and lax.ppermute only.
A program may use at most 64 MiB of HBM per device.

v0:
```python
import jax
import jax.numpy as jnp
from jax import lax
from jax.sharding import PartitionSpec as P

EPS = 1e-06


def from_everyone(shard, axis):
    copies = jnp.broadcast_to(shard, (lax.axis_size(axis), *shard.shape))
    return lax.all_to_all(copies, axis, split_axis=0, concat_axis=0, tiled=True)


def joined_along(parts, dim):
    parts = jnp.moveaxis(parts, 0, dim)
    shape = parts.shape
    return parts.reshape(*shape[:dim], shape[dim] * shape[dim + 1], *shape[dim + 2 :])


def collect(shard, axis, dim):
    parts = from_everyone(shard, axis)
    return joined_along(parts, dim)


def local(tokens, norm_gain, w_in, w_out):
    xf = tokens.astype(jnp.float32)
    scale = lax.rsqrt(jnp.mean(xf * xf, axis=-1, keepdims=True) + EPS)
    normed = (xf * scale * norm_gain).astype(jnp.bfloat16)
    whole_in = lax.all_gather(w_in, "fs", axis=0, tiled=True)
    pre = jnp.dot(collect(normed, "tp", 0), whole_in, preferred_element_type=jnp.float32)
    hidden = jnp.square(jax.nn.relu(pre)).astype(jnp.bfloat16)
    whole_out = lax.all_gather(w_out, "fs", axis=1, tiled=True)
    summed = lax.psum_scatter(
        jnp.dot(hidden, whole_out, preferred_element_type=jnp.float32).astype(jnp.bfloat16),
        "tp",
        scatter_dimension=0,
        tiled=True,
    ).astype(jnp.float32)
    return (xf + summed).astype(jnp.bfloat16)


def solution(mesh):
    in_specs = (P(("grp", "fs", "tp"), None), P(), P("fs", "tp"), P("tp", "fs"))
    out_specs = P(("grp", "fs", "tp"), None)
    return jax.shard_map(local, mesh=mesh, in_specs=in_specs, out_specs=out_specs, check_vma=False)
```

profile of v0, /device:TPU:40, one launch (start us, length us, event | category | flops | bytes accessed | tf_op | source)
XLA Modules:
  0.0 253.1 jit_solution(16195759570042781914)
XLA Ops:
  6.5 0.0 all-gather.3.cloned.1.call-start
  6.6 0.7 all-gather.3.cloned.1.call-update
  7.3 0.1 all-gather.5.cloned.1.call-start
  7.4 0.7 all-gather.5.cloned.1.call-update
  8.1 0.1 reduce-scatter.2.cloned.1.call-start
  8.2 1.2 fusion
  9.4 1.2 fusion.2
  10.7 0.5 broadcast_in_dim.2
  11.2 54.2 %all_to_all.5 = bf16[8,128,2048]{2,1,0:T(8,128)(2,1)} all-to-all(bf16[8,128,2048]{2,1,0:T(8,128)(2,1)S(1)} %broadcast_in_dim.2), channel_id=1, replica_groups=mesh['grp'=2,'fs'=16,'tp'=8] {'tp'}, dimensions={0} | all-to-all | bytes 8388608 | tf_op jit(solution)/shard_map/all_to_all | solution.py:11
  65.4 33.0 %all-gather.3.cloned.1.call-done = bf16[2048,1024]{1,0:T(8,128)(2,1)} async-done(((bf16[128,1024]{1,0:T(8,128)(2,1)}), bf16[2048,1024]{1,0:T(8,128)(2,1)}) %all-gather.3.cloned.1.call-update) | async-done | bytes 4194320 | tf_op jit(solution)/shard_map/all_gather | solution.py:29
  98.3 91.3 %all-gather.5.cloned.1.call-done = bf16[1024,2048]{1,0:T(8,128)(2,1)} async-done(((bf16[1024,128]{1,0:T(8,128)(2,1)}), bf16[1024,2048]{1,0:T(8,128)(2,1)}) %all-gather.5.cloned.1.call-update) | async-done | bytes 4194320 | tf_op jit(solution)/shard_map/all_gather | solution.py:32
  189.6 14.4 %convolution_convert_fusion = bf16[1024,2048]{1,0:T(8,128)(2,1)} fusion(bf16[1024,2048]{1,0:T(8,128)(2,1)} %all-gather.5.cloned.1.call-done, bf16[1024,2048]{1,0:T(8,128)(2,1)} %bitcast.4, bf16[2048,1024]{1,0:T(8,128)(2,1)} %all-gather.3.cloned.1.call-done), kind=kOutput, calls=%fused_computation.1 | convolution fusion | flops 8595177472 | bytes 16777216 | tf_op jit(solution)/shard_map/dot_general | solution.py:34
  204.0 0.0 copy-start
  204.0 0.1 reduce-scatter.2.cloned.1.call-update
  204.1 40.5 %reduce-scatter.2.cloned.1.call-done = bf16[128,2048]{1,0:T(8,128)(2,1)} async-done(((bf16[1024,2048]{1,0:T(8,128)(2,1)}), bf16[128,2048]{1,0:T(8,128)(2,1)}) %reduce-scatter.2.cloned.1.call-update) | async-done | bytes 524304 | tf_op jit(solution)/shard_map/reduce_scatter | solution.py:33
  244.5 0.0 copy-done
  244.5 2.0 fusion.3
  (1 shorter events, 0.0 us)
Async XLA Ops:
  6.5 91.8 %all-gather.3.cloned.1.call-start = ((), (), s32[]{:S(2)}) async-start(), calls=%async_computation.2 | async-start | bytes 4456448 | tf_op jit(solution)/shard_map/all_gather | solution.py:29
  7.3 182.3 %all-gather.5.cloned.1.call-start = ((), (), s32[]{:S(2)}) async-start(), calls=%async_computation.3 | async-start | bytes 4456448 | tf_op jit(solution)/shard_map/all_gather | solution.py:32
  8.1 236.4 %reduce-scatter.2.cloned.1.call-start = ((), (), s32[]{:S(2)}) async-start(), calls=%async_computation.4 | async-start | bytes 4718592 | tf_op jit(solution)/shard_map/reduce_scatter | solution.py:33
  204.0 40.6 %copy-start = (bf16[128,2048]{1,0:T(8,128)(2,1)S(1)}, bf16[128,2048]{1,0:T(8,128)(2,1)}, u32[]{:S(2)}) copy-start(bf16[128,2048]{1,0:T(8,128)(2,1)} %param.4) | copy-start | bytes 1572868
Sparse Core Ops, SparseCore 0:
  9.1 89.1 all-gather.2
  100.1 89.5 all-gather.4
  204.2 40.3 reduce-scatter.1
where the time goes:
time: 253 us
  waiting for transfers between devices  166 us (66%)
  blocking collectives  54.2 us (21%)
  matrix products  14.4 us (6%)
  between operations  13.1 us (5%)
  other arithmetic  4.44 us (2%)
    all_gather x1, waiting for transfers between devices, local(): whole_out = lax.all_gather(w_out, 'fs', axis=1, tiled=True)  91.3 us
    all_to_all x1, blocking collectives, from_everyone(): return lax.all_to_all(copies, axis, split_axis=0, concat_axis=0, tiled=True)  54.2 us
    reduce_scatter x1, waiting for transfers between devices, local(): lax.psum_scatter(jnp.dot(hidden, whole_out, preferred_element_type=jnp.fl...  40.5 us
    all_gather x1, waiting for transfers between devices, local(): whole_in = lax.all_gather(w_in, 'fs', axis=0, tiled=True)  33 us
    dot_general x1, matrix products, local(): jnp.dot(hidden, whole_out, preferred_element_type=jnp.float32)  14.4 us
  transfers between devices with their start and end apart: 3, of which 3 were waited for; matrix products, arithmetic and copies ran while one was open for 1% of the time, Pallas kernels for 0%

commit v1 on v0

--- a/solution.py
+++ b/solution.py
@@ -26,7 +26,11 @@
     xf = tokens.astype(jnp.float32)
     scale = lax.rsqrt(jnp.mean(xf * xf, axis=-1, keepdims=True) + EPS)
     normed = (xf * scale * norm_gain).astype(jnp.bfloat16)
-    whole_in = lax.all_gather(w_in, "fs", axis=0, tiled=True)
+    length = lax.axis_size("fs")
+    repeats = [length if d == 0 else 1 for d in range(w_in.ndim)]
+    whole_in = lax.all_to_all(
+        jnp.tile(w_in, repeats), "fs", split_axis=0, concat_axis=0, tiled=True
+    )
     pre = jnp.dot(collect(normed, "tp", 0), whole_in, preferred_element_type=jnp.float32)
     hidden = jnp.square(jax.nn.relu(pre)).astype(jnp.bfloat16)
     whole_out = lax.all_gather(w_out, "fs", axis=1, tiled=True)

time: 253 us -> 394 us (1.56)
  waiting for transfers between devices: 166 us -> 280 us
  starting transfers between devices: 0.13 us -> 24.1 us
    all_gather x1, waiting for transfers between devices: 91.3 us -> 239 us  [local(): whole_out = lax.all_gather(w_out, 'fs', axis=1, tiled=True)]
    all_gather x1 -> x0, waiting for transfers between devices: 33 us -> none  [local(): whole_in = lax.all_gather(w_in, 'fs', axis=0, tiled=True)]
    all_to_all x0 -> x1, starting transfers between devices: none -> 24 us  [local(): lax.all_to_all(jnp.tile(w_in, repeats), 'fs', split_axis=0, concat_axis=0...]
  transfers between devices with their start and end apart: 3 -> 3, of which waited for: 3 -> 2; matrix products, arithmetic and copies ran while one was open for 1% -> 0% of each run, Pallas kernels for 0% -> 0%
where the time goes in v1:
time: 394 us
  waiting for transfers between devices  280 us (71%)
  blocking collectives  54.3 us (14%)
  starting transfers between devices  24.1 us (6%)
  matrix products  14.4 us (4%)
  between operations  13.5 us (3%)
  other arithmetic  4.44 us (1%)
    all_gather x1, waiting for transfers between devices, local(): whole_out = lax.all_gather(w_out, 'fs', axis=1, tiled=True)  239 us
    all_to_all x1, blocking collectives, from_everyone(): return lax.all_to_all(copies, axis, split_axis=0, concat_axis=0, tiled=True)  54.3 us
    reduce_scatter x1, waiting for transfers between devices, local(): lax.psum_scatter(jnp.dot(hidden, whole_out, preferred_element_type=jnp.fl...  39.9 us
    all_to_all x1, starting transfers between devices, local(): lax.all_to_all(jnp.tile(w_in, repeats), 'fs', split_axis=0, concat_axis=0...  24 us
    dot_general x1, matrix products, local(): jnp.dot(hidden, whole_out, preferred_element_type=jnp.float32)  14.4 us
  transfers between devices with their start and end apart: 3, of which 2 were waited for; matrix products, arithmetic and copies ran while one was open for 0% of the time, Pallas kernels for 0%

profile of v1, /device:TPU:40, one launch (start us, length us, event | category | flops | bytes accessed | tf_op | source)
XLA Modules:
  0.0 393.8 jit_solution(1049167812573036667)
XLA Ops:
  6.5 1.2 fusion
  7.8 1.2 fusion.2
  9.0 0.5 broadcast_in_dim.2
  9.6 0.0 copy-start.1
  9.6 54.3 %all_to_all.14 = bf16[8,128,2048]{2,1,0:T(8,128)(2,1)} all-to-all(bf16[8,128,2048]{2,1,0:T(8,128)(2,1)S(1)} %broadcast_in_dim.2), channel_id=1, replica_groups=mesh['grp'=2,'fs'=16,'tp'=8] {'tp'}, dimensions={0} | all-to-all | bytes 8388608 | tf_op jit(solution)/shard_map/all_to_all | solution.py:11
  63.9 0.0 copy-done.1
  63.9 2.5 tile.2
  66.3 24.0 %all-to-all-start.1 = ((bf16[16,128,1024]{2,1,0:T(8,128)(2,1)}), bf16[16,128,1024]{2,1,0:T(8,128)(2,1)}, u32[]{:S(2)}, u32[]{:S(2)}) async-start(bf16[16,128,1024]{2,1,0:T(8,128)(2,1)} %tile.2), calls=%async_computation.1 | async-start | bytes 8388608 | tf_op jit(solution)/shard_map/all_to_all | solution.py:31
  90.3 0.1 all-gather.2.cloned.1.call-start
  90.4 0.7 all-gather.2.cloned.1.call-update
  91.1 0.1 reduce-scatter.2.cloned.1.call-start
  91.2 239.5 %all-gather.2.cloned.1.call-done = bf16[1024,2048]{1,0:T(8,128)(2,1)} async-done(((bf16[1024,128]{1,0:T(8,128)(2,1)}), bf16[1024,2048]{1,0:T(8,128)(2,1)}) %all-gather.2.cloned.1.call-update) | async-done | bytes 4194320 | tf_op jit(solution)/shard_map/all_gather | solution.py:36
  330.7 0.0 all-to-all-done.1
  330.7 14.4 %convolution_convert_fusion = bf16[1024,2048]{1,0:T(8,128)(2,1)} fusion(bf16[1024,2048]{1,0:T(8,128)(2,1)} %all-gather.2.cloned.1.call-done, bf16[1024,2048]{1,0:T(8,128)(2,1)} %bitcast.5, bf16[2048,1024]{1,0:T(8,128)(2,1)} %bitcast.1), kind=kOutput, calls=%fused_computation.1 | convolution fusion | flops 8595177472 | bytes 16777216 | tf_op jit(solution)/shard_map/dot_general | solution.py:38
  345.0 0.0 copy-start
  345.1 0.1 reduce-scatter.2.cloned.1.call-update
  345.1 39.9 %reduce-scatter.2.cloned.1.call-done = bf16[128,2048]{1,0:T(8,128)(2,1)} async-done(((bf16[1024,2048]{1,0:T(8,128)(2,1)}), bf16[128,2048]{1,0:T(8,128)(2,1)}) %reduce-scatter.2.cloned.1.call-update) | async-done | bytes 524304 | tf_op jit(solution)/shard_map/reduce_scatter | solution.py:37
  385.0 0.0 copy-done
  385.0 2.0 fusion.3
  (1 shorter events, 0.0 us)
Async XLA Ops:
  9.6 54.3 %copy-start.1 = (bf16[128,1024]{1,0:T(8,128)(2,1)S(1)}, bf16[128,1024]{1,0:T(8,128)(2,1)}, u32[]{:S(2)}) copy-start(bf16[128,1024]{1,0:T(8,128)(2,1)} %param.6) | copy-start | bytes 786436
  66.3 264.3 %all-to-all-start.1 = ((bf16[16,128,1024]{2,1,0:T(8,128)(2,1)}), bf16[16,128,1024]{2,1,0:T(8,128)(2,1)}, u32[]{:S(2)}, u32[]{:S(2)}) async-start(bf16[16,128,1024]{2,1,0:T(8,128)(2,1)} %tile.2), calls=%async_computation.1 | async-start | bytes 8388608 | tf_op jit(solution)/shard_map/all_to_all | solution.py:31
  90.3 240.4 %all-gather.2.cloned.1.call-start = ((), (), s32[]{:S(2)}) async-start(), calls=%async_computation.3 | async-start | bytes 4456448 | tf_op jit(solution)/shard_map/all_gather | solution.py:36
  91.1 293.9 %reduce-scatter.2.cloned.1.call-start = ((), (), s32[]{:S(2)}) async-start(), calls=%async_computation.4 | async-start | bytes 4718592 | tf_op jit(solution)/shard_map/reduce_scatter | solution.py:37
  345.0 40.0 %copy-start = (bf16[128,2048]{1,0:T(8,128)(2,1)S(1)}, bf16[128,2048]{1,0:T(8,128)(2,1)}, u32[]{:S(2)}) copy-start(bf16[128,2048]{1,0:T(8,128)(2,1)} %param.4) | copy-start | bytes 1572868
Sparse Core Ops, SparseCore 0:
  92.9 237.7 all-gather.1
  345.2 39.7 reduce-scatter.1

commit v2 on v0

--- a/solution.py
+++ b/solution.py
@@ -29,7 +29,9 @@
     whole_in = lax.all_gather(w_in, "fs", axis=0, tiled=True)
     pre = jnp.dot(collect(normed, "tp", 0), whole_in, preferred_element_type=jnp.float32)
     hidden = jnp.square(jax.nn.relu(pre)).astype(jnp.bfloat16)
-    whole_out = lax.all_gather(w_out, "fs", axis=1, tiled=True)
+    whole_out = jnp.concatenate(
+        lax.all_to_all(jnp.stack([w_out] * lax.axis_size("fs")), "fs", 0, 0), axis=1
+    )
     summed = lax.psum_scatter(
         jnp.dot(hidden, whole_out, preferred_element_type=jnp.float32).astype(jnp.bfloat16),
         "tp",

time: 253 us -> 384 us (1.52)
  waiting for transfers between devices: 166 us -> 318 us
  blocking collectives: 54.2 us -> 0 us
  starting transfers between devices: 0.13 us -> 29 us
  local copies, waits for them, and re-layouts: 0.52 us -> 5.13 us
    all_gather x1, waiting for transfers between devices: 33 us -> 227 us  [local(): whole_in = lax.all_gather(w_in, 'fs', axis=0, tiled=True)]
    all_gather x1 -> x0, waiting for transfers between devices: 91.3 us -> none  [local(): whole_out = lax.all_gather(w_out, 'fs', axis=1, tiled=True)]
    all_to_all x1 -> x0, blocking collectives: 54.2 us -> none  [from_everyone(): return lax.all_to_all(copies, axis, split_axis=0, concat_axis=0, tiled=True)]
    all_to_all x0 -> x2, waiting for transfers between devices: none -> 49.4 us  [the longest x1 49.4 us: from_everyone(): return lax.all_to_all(copies, axis, split_axis=0, concat_axis=0, tiled=True)]
    all_to_all x0 -> x2, starting transfers between devices: none -> 28.8 us  [the longest x1 24 us: local(): lax.all_to_all(jnp.stack([w_out] * lax.axis_size('fs')), 'fs', 0, 0)]
  transfers between devices with their start and end apart: 3 -> 4, of which waited for: 3 -> 3; matrix products, arithmetic and copies ran while one was open for 1% -> 0% of each run, Pallas kernels for 0% -> 0%
where the time goes in v2:
time: 384 us
  waiting for transfers between devices  318 us (83%)
  starting transfers between devices  29 us (8%)
  matrix products  14.4 us (4%)
  between operations  13.5 us (4%)
  local copies, waits for them, and re-layouts  5.13 us (1%)
  other arithmetic  4.44 us (1%)
    all_gather x1, waiting for transfers between devices, local(): whole_in = lax.all_gather(w_in, 'fs', axis=0, tiled=True)  227 us
    all_to_all x1, waiting for transfers between devices, from_everyone(): return lax.all_to_all(copies, axis, split_axis=0, concat_axis=0, tiled=True)  49.4 us
    reduce_scatter x1, waiting for transfers between devices, local(): lax.psum_scatter(jnp.dot(hidden, whole_out, preferred_element_type=jnp.fl...  40.1 us
    all_to_all x1, starting transfers between devices, local(): lax.all_to_all(jnp.stack([w_out] * lax.axis_size('fs')), 'fs', 0, 0)  24 us
    dot_general x1, matrix products, local(): jnp.dot(hidden, whole_out, preferred_element_type=jnp.float32)  14.4 us
  transfers between devices with their start and end apart: 4, of which 3 were waited for; matrix products, arithmetic and copies ran while one was open for 0% of the time, Pallas kernels for 0%

profile of v2, /device:TPU:40, one launch (start us, length us, event | category | flops | bytes accessed | tf_op | source)
XLA Modules:
  0.0 383.9 jit_solution(15606499029884411505)
XLA Ops:
  6.5 1.2 fusion
  7.8 1.2 fusion.2
  9.0 2.5 broadcast_in_dim.2
  11.5 0.0 copy-start.1
  11.5 4.9 %all-to-all-start = ((bf16[8,128,2048]{2,1,0:T(8,128)(2,1)}), bf16[8,128,2048]{2,1,0:T(8,128)(2,1)}, u32[]{:S(2)}, u32[]{:S(2)}) async-start(bf16[8,128,2048]{2,1,0:T(8,128)(2,1)} %broadcast_in_dim.2), calls=%async_computation | async-start | bytes 8388608 | tf_op jit(solution)/shard_map/all_to_all | solution.py:11
  16.4 0.0 copy-done.1
  16.4 0.1 copy.5
  16.6 49.4 %all-to-all-done = bf16[8,128,2048]{2,1,0:T(8,128)(2,1)} async-done(((bf16[8,128,2048]{2,1,0:T(8,128)(2,1)}), bf16[8,128,2048]{2,1,0:T(8,128)(2,1)}, u32[]{:S(2)}, u32[]{:S(2)}) %all-to-all-start) | async-done | bytes 4194336 | tf_op jit(solution)/shard_map/all_to_all | solution.py:11
  66.0 2.5 stack.2
  68.5 24.0 %all-to-all-start.1 = ((bf16[16,1024,128]{1,2,0:T(8,128)(2,1)}), bf16[16,1024,128]{1,2,0:T(8,128)(2,1)}, u32[]{:S(2)}, u32[]{:S(2)}) async-start(bf16[16,1024,128]{1,2,0:T(8,128)(2,1)} %stack.2), calls=%async_computation.1 | async-start | bytes 8388608 | tf_op jit(solution)/shard_map/all_to_all | solution.py:33
  92.5 0.1 all-gather.2.cloned.1.call-start
  92.5 0.7 all-gather.2.cloned.1.call-update
  93.3 0.1 reduce-scatter.2.cloned.1.call-start
  93.3 227.2 %all-gather.2.cloned.1.call-done = bf16[2048,1024]{1,0:T(8,128)(2,1)} async-done(((bf16[128,1024]{1,0:T(8,128)(2,1)}), bf16[2048,1024]{1,0:T(8,128)(2,1)}) %all-gather.2.cloned.1.call-update) | async-done | bytes 4194320 | tf_op jit(solution)/shard_map/all_gather | solution.py:29
  320.5 0.0 all-to-all-done.1
  320.5 14.4 %convolution_convert_fusion = bf16[1024,2048]{1,0:T(8,128)(2,1)} fusion(bf16[1024,2048]{0,1:T(8,128)(2,1)} %bitcast.2, bf16[1024,2048]{1,0:T(8,128)(2,1)} %bitcast, bf16[2048,1024]{1,0:T(8,128)(2,1)} %all-gather.2.cloned.1.call-done), kind=kOutput, calls=%fused_computation.1 | convolution fusion | flops 8595177472 | bytes 16777216 | tf_op jit(solution)/shard_map/dot_general | solution.py:36
  334.9 0.0 copy-start
  334.9 0.1 reduce-scatter.2.cloned.1.call-update
  335.0 40.1 %reduce-scatter.2.cloned.1.call-done = bf16[128,2048]{1,0:T(8,128)(2,1)} async-done(((bf16[1024,2048]{1,0:T(8,128)(2,1)}), bf16[128,2048]{1,0:T(8,128)(2,1)}) %reduce-scatter.2.cloned.1.call-update) | async-done | bytes 524304 | tf_op jit(solution)/shard_map/reduce_scatter | solution.py:35
  375.1 0.0 copy-done
  375.1 2.0 fusion.3
  (1 shorter events, 0.0 us)
Async XLA Ops:
  11.5 4.9 %copy-start.1 = (bf16[1024,128]{1,0:T(8,128)(2,1)S(1)}, bf16[1024,128]{1,0:T(8,128)(2,1)}, u32[]{:S(2)}) copy-start(bf16[1024,128]{1,0:T(8,128)(2,1)} %param.7) | copy-start | bytes 786436
  11.5 54.5 %all-to-all-start = ((bf16[8,128,2048]{2,1,0:T(8,128)(2,1)}), bf16[8,128,2048]{2,1,0:T(8,128)(2,1)}, u32[]{:S(2)}, u32[]{:S(2)}) async-start(bf16[8,128,2048]{2,1,0:T(8,128)(2,1)} %broadcast_in_dim.2), calls=%async_computation | async-start | bytes 8388608 | tf_op jit(solution)/shard_map/all_to_all | solution.py:11
  68.5 252.1 %all-to-all-start.1 = ((bf16[16,1024,128]{1,2,0:T(8,128)(2,1)}), bf16[16,1024,128]{1,2,0:T(8,128)(2,1)}, u32[]{:S(2)}, u32[]{:S(2)}) async-start(bf16[16,1024,128]{1,2,0:T(8,128)(2,1)} %stack.2), calls=%async_computation.1 | async-start | bytes 8388608 | tf_op jit(solution)/shard_map/all_to_all | solution.py:33
  92.5 228.1 %all-gather.2.cloned.1.call-start = ((), (), s32[]{:S(2)}) async-start(), calls=%async_computation.3 | async-start | bytes 4456448 | tf_op jit(solution)/shard_map/all_gather | solution.py:29
  93.3 281.8 %reduce-scatter.2.cloned.1.call-start = ((), (), s32[]{:S(2)}) async-start(), calls=%async_computation.4 | async-start | bytes 4718592 | tf_op jit(solution)/shard_map/reduce_scatter | solution.py:35
  334.9 40.2 %copy-start = (bf16[128,2048]{1,0:T(8,128)(2,1)S(1)}, bf16[128,2048]{1,0:T(8,128)(2,1)}, u32[]{:S(2)}) copy-start(bf16[128,2048]{1,0:T(8,128)(2,1)} %param.4) | copy-start | bytes 1572868
Sparse Core Ops, SparseCore 0:
  95.1 225.3 all-gather.1
  335.1 39.9 reduce-scatter.1
